TPU v7x, 256 devices: a whole 4x4x8 slice. The times are simulated.
256 devices in a mesh: gr: 2 (over z_hi), sp: 16 (over z_lo, y), tp: 8 (over x, core).
Axes of the slice: x: 4, y: 4, z: 8 (z_hi: 2, z_lo: 4; z = z_hi * 4 + z_lo), core: 2. Of those that a mesh axis runs over, the one named last changes fastest.
Arguments:
- tokens: bfloat16 [8, 8, 2048, 4096], P('gr', 'tp', 'sp'), may hold values from -6 to 6
- ln_gain: bfloat16 [4096], replicated, may hold values from 0.099609375 to 1.8984375
- w_key: bfloat16 [4096, 256], P('sp'), may hold values from -0.09375 to 0.09375
- w_value: bfloat16 [4096, 256], P('sp'), may hold values from -0.09375 to 0.09375
- queries: bfloat16 [32, 512], P(('gr', 'sp')), may hold values from -6 to 6
- head_shift: float32 [4, 8], replicated
- key_shift: float32 [32, 16384], P(('gr', 'sp'), 'tp')
Outputs:
- kv_cache: bfloat16 [32, 16384, 128], P(('gr', 'sp'), 'tp')
- first_read: float32 [32, 512], P(('gr', 'sp'))
All inputs are finite; a program needn't handle non-finite values.
Results may differ from a plain program's by a relative error of at most 0.0064.
Values may be sent and summed in bfloat16 or wider, within the bound.
A program may use at most 64 MiB of HBM per device.

v0:
```python
import math
import jax
import jax.numpy as jnp
from jax import lax
from jax.sharding import Mesh
from jax.sharding import PartitionSpec as P

HD = 64
KVH = 4
GROUP = 8
SP = ("sp_0", "sp_1")
GR_SP = ("gr", "sp_0", "sp_1")
epsilon = 1e-05


def in_order(pieces, dim):
    pieces = jnp.moveaxis(pieces, 0, dim)
    shape = pieces.shape
    return pieces.reshape(*shape[:dim], shape[dim] * shape[dim + 1], *shape[dim + 2 :])


def stacked_from(shard, axes, sequence):
    pieces = shard[None]
    for k in sequence:
        pieces = lax.all_gather(pieces, axes[k], axis=0, tiled=True)
    carried = [lax.axis_size(axes[k]) for k in reversed(sequence)]
    pieces = pieces.reshape(*carried, *shard.shape)
    turned = sorted(range(len(sequence)), key=lambda place: sequence[len(sequence) - 1 - place])
    return pieces.transpose(*turned, *range(len(sequence), pieces.ndim)).reshape(-1, *shard.shape)


def whole_of(shard, axes, sequence, dim):
    return in_order(stacked_from(shard, axes, sequence), dim)


def side_by_side(arrays, axis, dim, along):
    widths = [math.prod(a.shape[along:]) for a in arrays]
    both = jnp.concatenate(
        [a.reshape(*a.shape[:along], w) for a, w in zip(arrays, widths)], axis=along
    )
    filled = lax.all_gather(both, axis, axis=dim, tiled=True)
    pieces = jnp.split(filled, [sum(widths[:k]) for k in range(1, len(widths))], axis=along)
    return tuple(
        (b.reshape(*filled.shape[:along], *a.shape[along:]) for a, b in zip(arrays, pieces))
    )


def add_columns(normed, segment):
    return jnp.dot(normed, segment, preferred_element_type=jnp.float32)


def local(tokens, ln_gain, w_key, w_value, queries, head_shift, key_shift):
    seq_count = tokens.shape[0]
    sub_count = tokens.shape[2]
    width = tokens.shape[3]
    flat_rows = tokens.reshape(seq_count * sub_count, width).astype(jnp.float32)
    row_mean = jnp.mean(flat_rows, axis=1, keepdims=True)
    centred = flat_rows - row_mean
    row_var = jnp.mean(centred * centred, axis=1, keepdims=True)
    normed = (centred * lax.rsqrt(row_var + epsilon) * ln_gain.astype(jnp.float32)).astype(
        jnp.bfloat16
    )
    keys = add_columns(normed, whole_of(w_key, SP, (0, 1), 0))
    values = add_columns(normed, whole_of(w_value, SP, (0, 1), 0))
    joined = jnp.concatenate(
        [
            keys.astype(jnp.bfloat16).reshape(seq_count, sub_count, KVH, HD),
            values.astype(jnp.bfloat16).reshape(seq_count, sub_count, KVH, HD),
        ],
        axis=3,
    )
    arranged = jnp.transpose(joined, (0, 2, 1, 3)).reshape(seq_count * KVH, sub_count, 2 * HD)
    cache_here = lax.all_to_all(arranged, SP, split_axis=0, concat_axis=1, tiled=True)
    own_keys = cache_here[0, :, :HD]
    own_values = cache_here[0, :, HD:]
    kv_head = lax.axis_index(SP) % KVH
    picker = (jnp.arange(KVH) == kv_head).astype(jnp.float32)
    head_row = jnp.sum(picker[:, None] * head_shift, axis=0)
    query = queries.reshape(GROUP, HD)
    logits = jnp.einsum("gd,jd->gj", query, own_keys, preferred_element_type=jnp.float32) * HD ** (
        -0.5
    )
    logits = logits + head_row[:, None] + key_shift[0][None, :]
    log_beta = jax.nn.log_sigmoid(logits)
    log_keep = log_beta - logits
    within = lax.cumsum(log_keep, axis=1, reverse=True) - log_keep
    local_weight = jnp.exp(log_beta + within).astype(jnp.bfloat16)
    section_part = jnp.dot(local_weight, own_values, preferred_element_type=jnp.float32)
    section_total = jnp.sum(log_keep, axis=1)
    all_totals, all_parts = side_by_side((section_total[None], section_part[None]), "tp", 0, 2)
    carry_all = lax.cumsum(all_totals, axis=0, reverse=True) - all_totals
    first_read = jnp.sum(jnp.exp(carry_all)[:, :, None] * all_parts, axis=0)
    return (cache_here, first_read.reshape(1, GROUP * HD))


def solution(mesh):
    split = Mesh(
        mesh.devices.reshape(mesh.shape["gr"], 4, 4, mesh.shape["tp"]), ("gr", "sp_0", "sp_1", "tp")
    )
    placed = (
        P("gr", "tp", SP, None),
        P(),
        P(SP, None),
        P(SP, None),
        P(GR_SP, None),
        P(),
        P(GR_SP, "tp"),
    )
    return jax.shard_map(
        local,
        mesh=split,
        in_specs=placed,
        out_specs=(P(GR_SP, "tp", None), P(GR_SP, None)),
        check_vma=False,
    )
```

profile of v0, /device:TPU:1, one launch (start us, length us, event | category | flops | bytes accessed | tf_op | source)
XLA Modules:
  0.0 156.6 jit_solution(1758660517415116715)
XLA Ops:
  7.2 0.0 all-gather.7.cloned.1.call-start
  7.2 17.0 %all-gather.1 = bf16[1024,256]{1,0:T(8,128)(2,1)} all-gather(bf16[256,256]{1,0:T(8,128)(2,1)} %param.10), channel_id=3, replica_groups=mesh['gr'=2,'sp_0'=4,'sp_1'=4,'tp'=8] {'sp_0'}, dimensions={0}, use_global_device_ids=true | all-gather | bytes 655360 | tf_op jit(solution)/shard_map/all_gather | solution.py:25
  24.2 0.0 all-gather.7.cloned.1.call-update
  24.3 0.0 all-gather.5.cloned.1.call-start
  24.3 13.4 %all-gather = bf16[1024,256]{1,0:T(8,128)(2,1)} all-gather(bf16[256,256]{1,0:T(8,128)(2,1)} %param.9), channel_id=2, replica_groups=mesh['gr'=2,'sp_0'=4,'sp_1'=4,'tp'=8] {'sp_0'}, dimensions={0}, use_global_device_ids=true | all-gather | bytes 655360 | tf_op jit(solution)/shard_map/all_gather | solution.py:25
  37.7 0.0 all-gather.5.cloned.1.call-update
  37.8 0.0 copy-start
  37.8 0.9 convert_element_type.34
  38.6 3.4 %convert_reduce_fusion = f32[4,128]{1,0:T(4,128)S(1)} fusion(bf16[4,1,128,4096]{3,2,1,0:T(8,128)(2,1)} %param.7), kind=kLoop, calls=%fused_computation.1 | loop fusion | flops 4193792 | bytes 4196352 | tf_op jit(solution)/shard_map/reduce_sum | solution.py:57
  42.1 0.0 copy-done
  42.1 1.2 fusion.2
  43.3 4.3 %fusion.4 = bf16[4,1,128,4096]{3,2,1,0:T(8,128)(2,1)} fusion(bf16[4,1,128,4096]{3,2,1,0:T(8,128)(2,1)S(1)} %copy-done, f32[4096]{0:T(1024)S(1)} %convert_element_type.34, f32[4,128]{1,0:T(4,128)S(1)} %add_rsqrt_fusion, f32[4,128]{1,0:T(4,128)S(1)} %broadcast_multiply_fusion), kind=kLoop, calls=%fused_computation.6 | loop fusion | flops 10485760 | bytes 8409088 | tf_op jit(solution)/shard_map/convert_element_type | solution.py:60
  47.6 12.9 %all-gather.7.cloned.1.call-done = bf16[16,256,256]{2,1,0:T(8,128)(2,1)} async-done(((bf16[4,256,256]{2,1,0:T(8,128)(2,1)}), bf16[16,256,256]{2,1,0:T(8,128)(2,1)}) %all-gather.7.cloned.1.call-update) | async-done | bytes 2097168 | tf_op jit(solution)/shard_map/all_gather | solution.py:25
  60.6 0.0 copy-start.1
  60.6 1.9 %copy.25 = bf16[4,4,256,256]{3,2,1,0:T(8,128)(2,1)S(1)} copy(bf16[4,4,256,256]{3,2,0,1:T(8,128)(2,1)} %bitcast.57) | data formatting | bytes 4194304 | tf_op jit(solution)/shard_map/transpose | solution.py:29
  62.4 0.9 copy-done.1
  63.4 1.2 convolution_convert_fusion
  64.6 0.1 copy.26
  64.8 0.1 reshape.121
  64.8 30.9 %all-gather.5.cloned.1.call-done = bf16[16,256,256]{2,1,0:T(8,128)(2,1)} async-done(((bf16[4,256,256]{2,1,0:T(8,128)(2,1)}), bf16[16,256,256]{2,1,0:T(8,128)(2,1)}) %all-gather.5.cloned.1.call-update) | async-done | bytes 2097168 | tf_op jit(solution)/shard_map/all_gather | solution.py:25
  95.8 0.0 copy-start.2
  95.8 1.9 %copy.23 = bf16[4,4,256,256]{3,2,1,0:T(8,128)(2,1)S(1)} copy(bf16[4,4,256,256]{3,2,0,1:T(8,128)(2,1)} %bitcast.56) | data formatting | bytes 4194304 | tf_op jit(solution)/shard_map/transpose | solution.py:29
  97.7 0.9 copy-done.2
  98.6 0.0 copy-start.3
  98.6 0.0 copy-start.4
  98.6 0.0 copy-start.5
  98.6 1.2 convolution_convert_fusion.1
  99.9 0.1 copy.24
  100.0 0.1 reshape.119
  100.1 0.3 maximum_bitcast_fusion
  100.4 1.1 copy.27
  101.5 5.8 %all-to-all-start = ((bf16[16,128,128]{2,1,0:T(8,128)(2,1)}), bf16[16,128,128]{2,1,0:T(8,128)(2,1)S(1)}, u32[]{:S(2)}, u32[]{:S(2)}) async-start(bf16[16,128,128]{2,1,0:T(8,128)(2,1)} %bitcast.10), calls=%async_computation | async-start | bytes 1048576 | tf_op jit(solution)/shard_map/all_to_all | solution.py:73
  107.4 0.0 copy-done.3
  107.4 0.1 reshape.123
  107.5 0.0 copy-done.4
  107.5 0.1 multiply_reduce_fusion
  107.6 13.4 %all-to-all-done = bf16[16,128,128]{2,1,0:T(8,128)(2,1)S(1)} async-done(((bf16[16,128,128]{2,1,0:T(8,128)(2,1)}), bf16[16,128,128]{2,1,0:T(8,128)(2,1)S(1)}, u32[]{:S(2)}, u32[]{:S(2)}) %all-to-all-start) | async-done | bytes 524320 | tf_op jit(solution)/shard_map/all_to_all | solution.py:73
  121.0 0.0 copy-done.5
  121.0 0.2 fusion.7
  121.3 0.2 fusion.18
  121.5 9.9 %reduce-window.6 = f32[8,16,128]{2,1,0:T(8,128)S(1)} reduce-window(f32[8,16,128]{2,1,0:T(8,128)S(1)} %copy.28, f32[]{:T(128)} %constant.30.clone.1), window={size=1x1x128 pad=0_0x0_0x0_127}, to_apply=%region_4.5 | reduce-window | flops 2080768 | bytes 131076 | tf_op jit(solution)/shard_map/reduce-window
  131.4 0.1 slice_reduce_fusion
  131.5 0.2 reduce-window.9
  131.7 0.1 slice.14
  131.8 0.1 add_bitcast_fusion
  131.8 0.3 convolution_bitcast_fusion
  132.2 0.1 copy.29
  132.3 0.1 pad_maximum_fusion
  132.3 15.7 %all_gather.19 = f32[8,8,65]{2,1,0:T(8,128)S(1)} all-gather(f32[1,8,65]{2,1,0:T(8,128)S(1)} %pad_maximum_fusion), channel_id=1, replica_groups=mesh['gr'=2,'sp_0'=4,'sp_1'=4,'tp'=8] {'tp'}, dimensions={0}, use_global_device_ids=true | all-gather | bytes 18720 | tf_op jit(solution)/shard_map/all_gather | solution.py:41
  148.0 0.1 copy.31
  148.2 0.1 fusion.14
  148.3 0.7 reshape.126
  149.0 0.8 copy.36
  (7 shorter events, 0.1 us)
Async XLA Ops:
  7.2 53.4 %all-gather.7.cloned.1.call-start = ((), (), s32[]{:S(2)}) async-start(), calls=%async_computation.2 | async-start | bytes 2621440 | tf_op jit(solution)/shard_map/all_gather | solution.py:25
  24.3 71.5 %all-gather.5.cloned.1.call-start = ((), (), s32[]{:S(2)}) async-start(), calls=%async_computation.1 | async-start | bytes 2621440 | tf_op jit(solution)/shard_map/all_gather | solution.py:25
  37.8 4.3 %copy-start = (bf16[4,1,128,4096]{3,2,1,0:T(8,128)(2,1)S(1)}, bf16[4,1,128,4096]{3,2,1,0:T(8,128)(2,1)}, u32[]{:S(2)}) copy-start(bf16[4,1,128,4096]{3,2,1,0:T(8,128)(2,1)} %param.7) | copy-start | bytes 12582916
  60.6 2.8 %copy-start.1 = (bf16[4,1,128,4096]{3,2,1,0:T(8,128)(2,1)S(1)}, bf16[4,1,128,4096]{3,2,1,0:T(8,128)(2,1)}, u32[]{:S(2)}) copy-start(bf16[4,1,128,4096]{3,2,1,0:T(8,128)(2,1)} %fusion.4) | copy-start | bytes 12582916
  95.8 2.8 %copy-start.2 = (bf16[4,1,128,4096]{3,2,1,0:T(8,128)(2,1)S(1)}, bf16[4,1,128,4096]{3,2,1,0:T(8,128)(2,1)}, u32[]{:S(2)}) copy-start(bf16[4,1,128,4096]{3,2,1,0:T(8,128)(2,1)} %fusion.4) | copy-start | bytes 12582916
  98.6 8.8 %copy-start.3 = (bf16[1,512]{1,0:T(2,128)(2,1)S(1)}, bf16[1,512]{1,0:T(2,128)(2,1)}, u32[]{:S(2)}) copy-start(bf16[1,512]{1,0:T(2,128)(2,1)} %param.11) | copy-start | bytes 3076
  98.6 8.9 %copy-start.4 = (f32[4,8]{1,0:T(4,128)S(1)}, f32[4,8]{1,0:T(4,128)}, u32[]{:S(2)}) copy-start(f32[4,8]{1,0:T(4,128)} %param.12) | copy-start | bytes 388
  98.6 22.4 %copy-start.5 = (f32[1,2048]{1,0:T(1,128)S(1)}, f32[1,2048]{1,0:T(1,128)}, u32[]{:S(2)}) copy-start(f32[1,2048]{1,0:T(1,128)} %param.13) | copy-start | bytes 24580
  101.5 19.5 %all-to-all-start = ((bf16[16,128,128]{2,1,0:T(8,128)(2,1)}), bf16[16,128,128]{2,1,0:T(8,128)(2,1)S(1)}, u32[]{:S(2)}, u32[]{:S(2)}) async-start(bf16[16,128,128]{2,1,0:T(8,128)(2,1)} %bitcast.10), calls=%async_computation | async-start | bytes 1048576 | tf_op jit(solution)/shard_map/all_to_all | solution.py:73
Sparse Core Ops, SparseCore 0:
  24.4 36.1 all-gather.6
  62.4 33.3 all-gather.4
where the time goes:
time: 157 us
  waiting for transfers between devices  57.3 us (36%)
  blocking collectives  46.2 us (29%)
  other arithmetic  20.9 us (13%)
  between operations  14.2 us (9%)
  local copies, waits for them, and re-layouts  9.08 us (6%)
  starting transfers between devices  5.9 us (4%)
  matrix products  3.04 us (2%)
    all_gather x2, waiting for transfers between devices, stacked_from(): pieces = lax.all_gather(pieces, axes[k], axis=0, tiled=True)  43.9 us
    all_gather x2, blocking collectives, stacked_from(): pieces = lax.all_gather(pieces, axes[k], axis=0, tiled=True)  30.5 us
    all_gather x1, blocking collectives, side_by_side(): filled = lax.all_gather(both, axis, axis=dim, tiled=True)  15.7 us
    all_to_all x1, waiting for transfers between devices, local(): lax.all_to_all(arranged, SP, split_axis=0, concat_axis=1, tiled=True)  13.4 us
    another operation x2, other arithmetic  10.1 us
    all_to_all x1, starting transfers between devices, local(): lax.all_to_all(arranged, SP, split_axis=0, concat_axis=1, tiled=True)  5.82 us
    convert_element_type x1, other arithmetic, local(): (centred * lax.rsqrt(row_var + epsilon) * ln_gain.astype(jnp.float32)).as...  4.3 us
    transpose x2, local copies, waits for them, and re-layouts, stacked_from(): pieces.transpose(*turned, *range(len(sequence), pieces.ndim))  3.76 us
  transfers between devices with their start and end apart: 3, of which 3 were waited for; matrix products, arithmetic and copies ran while one was open for 9% of the time, Pallas kernels for 0%

commit v1 on v0

--- a/solution.py
+++ b/solution.py
@@ -70,7 +70,9 @@
         axis=3,
     )
     arranged = jnp.transpose(joined, (0, 2, 1, 3)).reshape(seq_count * KVH, sub_count, 2 * HD)
-    cache_here = lax.all_to_all(arranged, SP, split_axis=0, concat_axis=1, tiled=True)
+    cache_here = jnp.concatenate(
+        lax.all_to_all(jnp.stack(jnp.split(arranged, lax.axis_size(SP), 0), 0), SP, 0, 0), 1
+    )
     own_keys = cache_here[0, :, :HD]
     own_values = cache_here[0, :, HD:]
     kv_head = lax.axis_index(SP) % KVH

time: 157 us -> 166 us (1.057)
  local copies, waits for them, and re-layouts: 9.08 us -> 18.2 us
    unnamed x14 -> x29, local copies, waits for them, and re-layouts: 2.79 us -> 12.1 us
  transfers between devices with their start and end apart: 3 -> 3, of which waited for: 3 -> 3; matrix products, arithmetic and copies ran while one was open for 9% -> 8% of each run, Pallas kernels for 0% -> 0%
where the time goes in v1:
time: 166 us
  waiting for transfers between devices  57.4 us (35%)
  blocking collectives  46.2 us (28%)
  other arithmetic  20.8 us (13%)
  local copies, waits for them, and re-layouts  18.2 us (11%)
  between operations  14.2 us (9%)
  starting transfers between devices  5.9 us (4%)
  matrix products  3.04 us (2%)
    all_gather x2, waiting for transfers between devices, stacked_from(): pieces = lax.all_gather(pieces, axes[k], axis=0, tiled=True)  43.9 us
    all_gather x2, blocking collectives, stacked_from(): pieces = lax.all_gather(pieces, axes[k], axis=0, tiled=True)  30.4 us
    all_gather x1, blocking collectives, side_by_side(): filled = lax.all_gather(both, axis, axis=dim, tiled=True)  15.7 us
    all_to_all x1, waiting for transfers between devices, local(): lax.all_to_all(jnp.stack(jnp.split(arranged, lax.axis_size(SP), 0), 0), S...  13.4 us
    unnamed x29, local copies, waits for them, and re-layouts  12.1 us
    another operation x2, other arithmetic  10.1 us
    all_to_all x1, starting transfers between devices, local(): lax.all_to_all(jnp.stack(jnp.split(arranged, lax.axis_size(SP), 0), 0), S...  5.82 us
    convert_element_type x1, other arithmetic, local(): (centred * lax.rsqrt(row_var + epsilon) * ln_gain.astype(jnp.float32)).as...  4.3 us
  transfers between devices with their start and end apart: 3, of which 3 were waited for; matrix products, arithmetic and copies ran while one was open for 8% of the time, Pallas kernels for 0%

profile of v1, /device:TPU:1, one launch (start us, length us, event | category | flops | bytes accessed | tf_op | source)
XLA Modules:
  0.0 165.8 jit_solution(400030235128817751)
XLA Ops:
  7.2 0.0 all-gather.5.cloned.1.call-start
  7.2 17.0 %all-gather = bf16[1024,256]{1,0:T(8,128)(2,1)} all-gather(bf16[256,256]{1,0:T(8,128)(2,1)} %param.9), channel_id=2, replica_groups=mesh['gr'=2,'sp_0'=4,'sp_1'=4,'tp'=8] {'sp_0'}, dimensions={0}, use_global_device_ids=true | all-gather | bytes 655360 | tf_op jit(solution)/shard_map/all_gather | solution.py:25
  24.2 0.0 all-gather.5.cloned.1.call-update
  24.3 0.0 all-gather.7.cloned.1.call-start
  24.3 13.4 %all-gather.1 = bf16[1024,256]{1,0:T(8,128)(2,1)} all-gather(bf16[256,256]{1,0:T(8,128)(2,1)} %param.10), channel_id=3, replica_groups=mesh['gr'=2,'sp_0'=4,'sp_1'=4,'tp'=8] {'sp_0'}, dimensions={0}, use_global_device_ids=true | all-gather | bytes 655360 | tf_op jit(solution)/shard_map/all_gather | solution.py:25
  37.7 0.0 all-gather.7.cloned.1.call-update
  37.7 0.0 copy-start
  37.8 0.9 convert_element_type.34
  38.6 3.4 %convert_reduce_fusion = f32[4,128]{1,0:T(4,128)S(1)} fusion(bf16[4,1,128,4096]{3,2,1,0:T(8,128)(2,1)} %param.7), kind=kLoop, calls=%fused_computation.1 | loop fusion | flops 4193792 | bytes 4196352 | tf_op jit(solution)/shard_map/reduce_sum | solution.py:57
  42.0 0.0 copy-done
  42.1 1.2 fusion.2
  43.3 4.3 %fusion.4 = bf16[4,1,128,4096]{3,2,1,0:T(8,128)(2,1)} fusion(bf16[4,1,128,4096]{3,2,1,0:T(8,128)(2,1)S(1)} %copy-done, f32[4096]{0:T(1024)S(1)} %convert_element_type.34, f32[4,128]{1,0:T(4,128)S(1)} %add_rsqrt_fusion, f32[4,128]{1,0:T(4,128)S(1)} %broadcast_multiply_fusion), kind=kLoop, calls=%fused_computation.6 | loop fusion | flops 10485760 | bytes 8409088 | tf_op jit(solution)/shard_map/convert_element_type | solution.py:60
  47.6 13.0 %all-gather.5.cloned.1.call-done = bf16[16,256,256]{2,1,0:T(8,128)(2,1)} async-done(((bf16[4,256,256]{2,1,0:T(8,128)(2,1)}), bf16[16,256,256]{2,1,0:T(8,128)(2,1)}) %all-gather.5.cloned.1.call-update) | async-done | bytes 2097168 | tf_op jit(solution)/shard_map/all_gather | solution.py:25
  60.6 1.9 %copy.38 = bf16[4,4,256,256]{3,2,1,0:T(8,128)(2,1)S(1)} copy(bf16[4,4,256,256]{3,2,0,1:T(8,128)(2,1)} %bitcast.137) | data formatting | bytes 4194304 | tf_op jit(solution)/shard_map/transpose | solution.py:29
  62.5 0.9 copy-done.1
  63.4 1.2 convolution_convert_fusion.1
  64.6 0.1 copy.39
  64.8 0.1 reshape.119
  64.9 30.9 %all-gather.7.cloned.1.call-done = bf16[16,256,256]{2,1,0:T(8,128)(2,1)} async-done(((bf16[4,256,256]{2,1,0:T(8,128)(2,1)}), bf16[16,256,256]{2,1,0:T(8,128)(2,1)}) %all-gather.7.cloned.1.call-update) | async-done | bytes 2097168 | tf_op jit(solution)/shard_map/all_gather | solution.py:25
  95.8 1.9 %copy.40 = bf16[4,4,256,256]{3,2,1,0:T(8,128)(2,1)S(1)} copy(bf16[4,4,256,256]{3,2,0,1:T(8,128)(2,1)} %bitcast.136) | data formatting | bytes 4194304 | tf_op jit(solution)/shard_map/transpose | solution.py:29
  97.7 0.9 copy-done.2
  98.6 1.2 convolution_convert_fusion
  99.9 0.0 copy-start.3
  99.9 0.0 copy-start.4
  99.9 0.0 copy-start.5
  99.9 0.1 copy.41
  100.0 0.1 reshape.121
  100.1 0.3 maximum_bitcast_fusion
  100.5 0.4 copy.42
  100.9 0.6 constant_dynamic-update-slice_fusion.15
  101.5 0.6 constant_dynamic-update-slice_fusion.14
  102.1 0.6 constant_dynamic-update-slice_fusion.13
  102.7 0.6 constant_dynamic-update-slice_fusion.12
  103.3 0.6 constant_dynamic-update-slice_fusion.11
  103.9 0.6 constant_dynamic-update-slice_fusion.10
  104.6 0.6 constant_dynamic-update-slice_fusion.9
  105.2 0.6 constant_dynamic-update-slice_fusion.8
  105.8 0.6 constant_dynamic-update-slice_fusion.7
  106.4 0.6 constant_dynamic-update-slice_fusion.6
  107.0 0.6 constant_dynamic-update-slice_fusion.5
  107.6 0.6 constant_dynamic-update-slice_fusion.4
  108.3 0.6 constant_dynamic-update-slice_fusion.3
  108.9 0.6 constant_dynamic-update-slice_fusion.2
  109.5 0.6 constant_dynamic-update-slice_fusion.1
  110.1 0.6 constant_dynamic-update-slice_fusion
  110.7 5.8 %all-to-all-start = ((bf16[16,1,128,128]{3,2,1,0:T(8,128)(2,1)}), bf16[16,1,128,128]{3,2,1,0:T(8,128)(2,1)S(1)}, u32[]{:S(2)}, u32[]{:S(2)}) async-start(bf16[16,1,128,128]{3,2,1,0:T(8,128)(2,1)} %constant_dynamic-update-slice_fusion), calls=%async_computation | async-start | bytes 1048576 | tf_op jit(solution)/shard_map/all_to_all | solution.py:74
  116.6 0.1 reshape.124
  116.7 0.1 multiply_reduce_fusion
  116.8 13.4 %all-to-all-done = bf16[16,1,128,128]{3,2,1,0:T(8,128)(2,1)S(1)} async-done(((bf16[16,1,128,128]{3,2,1,0:T(8,128)(2,1)}), bf16[16,1,128,128]{3,2,1,0:T(8,128)(2,1)S(1)}, u32[]{:S(2)}, u32[]{:S(2)}) %all-to-all-start) | async-done | bytes 524320 | tf_op jit(solution)/shard_map/all_to_all | solution.py:74
  130.2 0.2 fusion.7
  130.5 0.2 fusion.18
  130.7 9.9 %reduce-window.6 = f32[8,16,128]{2,1,0:T(8,128)S(1)} reduce-window(f32[8,16,128]{2,1,0:T(8,128)S(1)} %copy.43, f32[]{:T(128)} %constant.30.clone.1), window={size=1x1x128 pad=0_0x0_0x0_127}, to_apply=%region_4.5 | reduce-window | flops 2080768 | bytes 131076 | tf_op jit(solution)/shard_map/reduce-window
  140.6 0.1 slice_reduce_fusion
  140.7 0.2 reduce-window.9
  140.9 0.1 slice.14
  140.9 0.1 add_bitcast_fusion
  141.0 0.3 convolution_bitcast_fusion
  141.4 0.1 copy.44
  141.4 0.1 pad_maximum_fusion
  141.5 15.7 %all_gather.19 = f32[8,8,65]{2,1,0:T(8,128)S(1)} all-gather(f32[1,8,65]{2,1,0:T(8,128)S(1)} %pad_maximum_fusion), channel_id=1, replica_groups=mesh['gr'=2,'sp_0'=4,'sp_1'=4,'tp'=8] {'tp'}, dimensions={0}, use_global_device_ids=true | all-gather | bytes 18720 | tf_op jit(solution)/shard_map/all_gather | solution.py:41
  157.2 0.1 copy.46
  157.4 0.1 fusion.14
  157.5 0.7 reshape.127
  158.2 0.8 copy.66
  (12 shorter events, 0.1 us)
Async XLA Ops:
  7.2 53.4 %all-gather.5.cloned.1.call-start = ((), (), s32[]{:S(2)}) async-start(), calls=%async_computation.1 | async-start | bytes 2621440 | tf_op jit(solution)/shard_map/all_gather | solution.py:25
  24.3 71.5 %all-gather.7.cloned.1.call-start = ((), (), s32[]{:S(2)}) async-start(), calls=%async_computation.2 | async-start | bytes 2621440 | tf_op jit(solution)/shard_map/all_gather | solution.py:25
  37.7 4.3 %copy-start = (bf16[4,1,128,4096]{3,2,1,0:T(8,128)(2,1)S(1)}, bf16[4,1,128,4096]{3,2,1,0:T(8,128)(2,1)}, u32[]{:S(2)}) copy-start(bf16[4,1,128,4096]{3,2,1,0:T(8,128)(2,1)} %param.7) | copy-start | bytes 12582916
  60.6 2.8 %copy-start.1 = (bf16[4,1,128,4096]{3,2,1,0:T(8,128)(2,1)S(1)}, bf16[4,1,128,4096]{3,2,1,0:T(8,128)(2,1)}, u32[]{:S(2)}) copy-start(bf16[4,1,128,4096]{3,2,1,0:T(8,128)(2,1)} %fusion.4) | copy-start | bytes 12582916
  95.8 2.8 %copy-start.2 = (bf16[4,1,128,4096]{3,2,1,0:T(8,128)(2,1)S(1)}, bf16[4,1,128,4096]{3,2,1,0:T(8,128)(2,1)}, u32[]{:S(2)}) copy-start(bf16[4,1,128,4096]{3,2,1,0:T(8,128)(2,1)} %fusion.4) | copy-start | bytes 12582916
  99.9 16.7 %copy-start.3 = (bf16[1,512]{1,0:T(2,128)(2,1)S(1)}, bf16[1,512]{1,0:T(2,128)(2,1)}, u32[]{:S(2)}) copy-start(bf16[1,512]{1,0:T(2,128)(2,1)} %param.11) | copy-start | bytes 3076
  99.9 16.8 %copy-start.4 = (f32[4,8]{1,0:T(4,128)S(1)}, f32[4,8]{1,0:T(4,128)}, u32[]{:S(2)}) copy-start(f32[4,8]{1,0:T(4,128)} %param.12) | copy-start | bytes 388
  99.9 30.3 %copy-start.5 = (f32[1,2048]{1,0:T(1,128)S(1)}, f32[1,2048]{1,0:T(1,128)}, u32[]{:S(2)}) copy-start(f32[1,2048]{1,0:T(1,128)} %param.13) | copy-start | bytes 24580
  110.7 19.5 %all-to-all-start = ((bf16[16,1,128,128]{3,2,1,0:T(8,128)(2,1)}), bf16[16,1,128,128]{3,2,1,0:T(8,128)(2,1)S(1)}, u32[]{:S(2)}, u32[]{:S(2)}) async-start(bf16[16,1,128,128]{3,2,1,0:T(8,128)(2,1)} %constant_dynamic-update-slice_fusion), calls=%async_computation | async-start | bytes 1048576 | tf_op jit(solution)/shard_map/all_to_all | solution.py:74
Sparse Core Ops, SparseCore 0:
  24.4 36.1 all-gather.4
  62.4 33.3 all-gather.6
